TPU v7x, 32 devices: a whole 2x2x4 slice. The times are simulated.
32 devices in a mesh: ep: 8 (over z, x), tp: 4 (over y, core).
Axes of the slice: x: 2, y: 2, z: 4, core: 2. Of those that a mesh axis runs over, the one named last changes fastest.
Arguments:
- queries: bfloat16 [4096, 1024], P('ep', 'tp'), may hold values from -6 to 6
- sequence_keys: bfloat16 [4096, 1024], P('ep', 'tp'), may hold values from -6 to 6
- stream_content_vectors: bfloat16 [4096, 2048], P('ep', 'tp'), may hold values from -6 to 6
- output_gate_logits: bfloat16 [4096, 2048], P('ep', 'tp'), may hold values from -6 to 6
- retention_preactivation: bfloat16 [4096, 1024], P('ep', 'tp'), may hold values from -3 to 10
- additional_fade_bias: float32 [4096, 1024], P('ep', 'tp'), may hold values from -2.1 to 0
- attention_group_rescale: float32 [128], replicated, may hold values from 0.1 to 1.9
- output_projection: bfloat16 [2048, 2048], P(None, 'tp'), may hold values from -0.125 to 0.125
- expert_batch_tokens: bfloat16 [1024, 2048], P('ep'), may hold values from -6 to 6
- expert_norm_gain: float32 [2048], replicated, may hold values from 0.1 to 1.9
- routed_expert_index: int32 [1024, 4], P('ep'), may hold values from 0 to 7, all different within a row; in each aligned block of 128 rows (0 to 127, 128 to 255, ...) at most 128 rows name the same one
- routed_expert_weights: float32 [1024, 4], P('ep'), may hold values from 0.2 to 1.2
- expert_gate_matrix: bfloat16 [8, 2048, 2048], P('ep', None, 'tp'), may hold values from -0.125 to 0.125
- expert_up_matrix: bfloat16 [8, 2048, 2048], P('ep', None, 'tp'), may hold values from -0.125 to 0.125
- expert_down_matrix: bfloat16 [8, 2048, 2048], P('ep', None, 'tp'), may hold values from -0.125 to 0.125
- shared_gate_matrix: bfloat16 [2048, 2048], P(None, 'tp'), may hold values from -0.125 to 0.125
- shared_up_matrix: bfloat16 [2048, 2048], P(None, 'tp'), may hold values from -0.125 to 0.125
- shared_down_matrix: bfloat16 [2048, 2048], P(None, 'tp'), may hold values from -0.125 to 0.125
Outputs:
- mixer_out: bfloat16 [4096, 2048], P('ep', 'tp')
- specialist_blend: bfloat16 [1024, 2048], P('ep', 'tp')
Inputs may be any that keep to these rules, and one draw needn't show every extreme that they name: `routed_expert_index`: each row names 4 different experts; among the rows of one index of ep no expert is named by more than 128 rows, a bound that some block reaches.
All inputs are finite; a program needn't handle non-finite values.
Results may differ from a plain program's by a relative error of at most 0.0069.
Values may be sent and summed in bfloat16 or wider, within the bound.
A program may use at most 64 MiB of HBM per device.

v0:
```python
import functools
import math

import jax
import jax.numpy as jnp
from jax import lax
from jax.experimental import pallas as pl
from jax.experimental.pallas import tpu as pltpu
from jax.sharding import PartitionSpec as P

DK = 64
DV = 128
BLOCK = 64
PAD = 16
CORES = 2
CH = 2

eps_norm = 1e-06
switch_softness = 16.0
bf16 = jnp.bfloat16
f32 = jnp.float32
NT = (((1,), (1,)), ((), ()))
TN = (((0,), (0,)), ((), ()))
MESH = pl.DeviceIdType.MESH


def silu(x):
    return x * jax.nn.sigmoid(x)


def dot(a, b):
    return jnp.dot(a, b, preferred_element_type=f32)


def body(sizes, *refs):
    Z, X, Y = sizes
    E, TP = Z * X, Y * CORES
    (
        q_hbm, k_hbm, v_hbm, og_hbm, r_hbm, b_hbm, gain_hbm, wo_hbm, tok_hbm, ng_hbm, idx_hbm, w_hbm,
        eg_hbm, eu_hbm, ed_hbm, sg_hbm, su_hbm, sd_hbm,
        mixer_hbm, blend_hbm,
        q_ref, k_ref, v_ref, og_ref, r_ref, b_ref, gain_ref, wo_ref, tok_ref, ng_ref, idx_ref, w_ref,
        eg_ref, eu_ref, ed_ref, sg_ref, su_ref, sd_ref,
        mixer_ref, blend_ref,
        R, GS, GE, GL, GH, RO, RI, A, B, mixed_ref, far_ref, state_ref, enter_ref, acc_ref,
        in_sem, out_sem,
        r_part_s, r_z_s, r_down_s, r_x_s, r_far_r, r_part_r,
        u_part_s, u_part_r, u_y_s, u_y_r, u_f_s, u_f_r,
        res_s, res_r, a_s, a_r, b_s, b_r,
    ) = refs

    ep, tp = lax.axis_index("ep"), lax.axis_index("tp")
    z, x = ep // X, ep % X
    y, c = tp // CORES, tp % CORES
    partner = y * CORES + (1 - c)
    rows = tok_ref.shape[0]
    seq, kw = q_ref.shape
    heads = kw // DK
    chunks = seq // rows
    width = GS.shape[-1]
    part = rows // (CH * CORES)

    def remote(src, dst, ssem, rsem, e, t):
        return pltpu.make_async_remote_copy(
            src_ref=src,
            dst_ref=dst,
            send_sem=ssem,
            recv_sem=rsem,
            device_id={"ep": e, "tp": t},
            device_id_type=MESH,
        )

    early = [
        (tok_hbm, tok_ref), (ng_hbm, ng_ref), (sg_hbm, sg_ref), (su_hbm, su_ref), (eg_hbm, eg_ref), (eu_hbm, eu_ref),
        (r_hbm, r_ref), (b_hbm, b_ref), (q_hbm, q_ref), (k_hbm, k_ref), (v_hbm, v_ref),
    ]
    late = [
        (sd_hbm, sd_ref), (ed_hbm, ed_ref), (og_hbm, og_ref), (gain_hbm, gain_ref), (wo_hbm, wo_ref),
        (idx_hbm, idx_ref), (w_hbm, w_ref),
    ]
    copies = {}

    def load(pairs):
        for n, (src, dst) in enumerate(pairs):
            copies[id(dst)] = pltpu.make_async_copy(src, dst, in_sem.at[n])
            copies[id(dst)].start()

    load(early)

    def need(*dsts):
        for dst in dsts:
            copies[id(dst)].wait()

    class Sends:
        def __init__(self, sems, count):
            self.sems, self.count, self.sent, self.held = sems, count, 0, {}

        def start(self, make):
            n = self.sent % self.count
            if n in self.held:
                self.held[n].wait_send()
            self.held[n] = make(self.sems.at[n])
            self.held[n].start()
            self.sent += 1

        def drain(self):
            for copy in self.held.values():
                copy.wait_send()

    barrier = pltpu.get_barrier_semaphore()

    def greet(e, t):
        pl.semaphore_signal(barrier, inc=1, device_id={"ep": e, "tp": t}, device_id_type=MESH)

    greet(ep, partner)
    for dy in range(1, Y):
        greet(ep, (y + dy) % Y * CORES + c)
    for dx in range(1, X):
        greet(z * X + (x + dx) % X, tp)
    pl.when(z < Z - 1)(lambda: greet(ep + X, tp))
    pl.when(z > 0)(lambda: greet(ep - X, tp))

    need(tok_ref, ng_ref)
    flat = tok_ref[...].astype(f32)
    normed = (
        flat * lax.rsqrt(jnp.mean(flat * flat, axis=-1, keepdims=True) + eps_norm) * ng_ref[...]
    ).astype(bf16)
    for n in range(CH * CORES):
        R[ep, n // CORES, n % CORES] = normed[n * part : (n + 1) * part]

    lines = jnp.where(z < Z - 1, 1, 0) + jnp.where(z > 0, 1, 0)
    pl.semaphore_wait(barrier, 1 + (Y - 1) + (X - 1) + lines)

    def row_part(b, h, kind=0):
        return remote(R.at[b, h, c], R.at[b, h, c], r_part_s.at[kind, h], r_part_r.at[b, h], ep, partner)

    def row_up(b, h):
        return remote(R.at[b, h, c], R.at[b, h, c], r_z_s.at[b // X, h], r_far_r.at[b, h], ep + X, tp)

    def row_down(b, h, sem=None):
        sem = r_z_s.at[b // X, h] if sem is None else sem
        return remote(R.at[b, h, c], R.at[b, h, c], sem, r_far_r.at[b, h], ep - X, tp)

    def row_x(b, h, dx):
        there = z * X + (x + dx) % X
        return remote(R.at[b, h, c], R.at[b, h, c], r_x_s.at[dx - 1, b // X, h], r_far_r.at[b, h], there, tp)

    def near(j):
        up = jnp.where(j <= Z - 1 - z, z + j, Z - 1 - j)
        down = jnp.where(j <= z, z - j, j)
        return jnp.where(2 * z < Z, up, down)

    def send_own(h):
        pl.when(z < Z - 1)(lambda: row_up(ep, h).start())
        pl.when(z > 0)(lambda: row_down(ep, h, r_down_s.at[h]).start())
        for dx in range(1, X):
            row_x(ep, h, dx).start()

    def arrive(b, h):
        remote(R.at[b, h, c], R.at[b, h, c], r_part_s.at[0, h], r_far_r.at[b, h], ep, partner).wait_recv()

    def hand_over(b, h, kind, again):
        copy = row_part(b, h, kind)
        if again:
            copy.wait_send()
        copy.start()

    def relay_line(k, h):
        @pl.when(z >= k)
        def _():
            b = ep - k * X
            arrive(b, h)
            pl.when(z < Z - 1)(lambda: row_up(b, h).start())
            hand_over(b, h, 0, k > 1)

        @pl.when(z + k < Z)
        def _():
            b = ep + k * X
            arrive(b, h)
            pl.when(z > 0)(lambda: row_down(b, h).start())
            hand_over(b, h, 1, k > 1)

        for dx in range(1, X):
            row_x(near(k) * X + x, h, dx).start()

    def relay_side(j, h, dx):
        b = near(j) * X + (x + dx) % X
        arrive(b, h)
        hand_over(b, h, 1 + dx, j > 0)

    def rows_of(b, h):
        return jnp.concatenate([R[b, h, n] for n in range(CORES)], axis=0)

    part_sends = Sends(u_part_s, u_part_s.shape[0])
    y_sends = [Sends(u_y_s.at[n], u_y_s.shape[1]) for n in range(Y - 1)]
    f_sends = [Sends(u_f_s.at[n], u_f_s.shape[1]) for n in range(Y - 1)]
    result_sends = Sends(res_s, res_s.shape[0])

    def unit_part(unit, sem=None):
        G, n, u = unit
        sem = u_part_s.at[0] if sem is None else sem
        return remote(G.at[n, tp], G.at[n, tp], sem, u_part_r.at[u], ep, partner)

    def unit_y(unit, dy, sem=None):
        G, n, u = unit
        t = (y + dy) % Y * CORES + c
        sem = u_y_s.at[dy - 1, 0] if sem is None else sem
        return remote(G.at[n, tp], G.at[n, tp], sem, u_y_r.at[dy - 1, u], ep, t)

    def unit_f(unit, dy, sem=None):
        G, n, u = unit
        t = (y - dy + Y) % Y * CORES + c
        sem = u_f_s.at[dy - 1, 0] if sem is None else sem
        return remote(G.at[n, t], G.at[n, t], sem, u_f_r.at[dy - 1, u], ep, partner)

    def unit_send(unit):
        for dy in range(1, Y):
            y_sends[dy - 1].start(lambda sem: unit_y(unit, dy, sem))
        part_sends.start(lambda sem: unit_part(unit, sem))

    def unit_forward(unit):
        for dy in range(1, Y):
            unit_y(unit, dy).wait_recv()
            f_sends[dy - 1].start(lambda sem: unit_f(unit, dy, sem))

    def unit_wait(unit):
        unit_part(unit).wait_recv()
        for dy in range(1, Y):
            unit_f(unit, dy).wait_recv()

    def unit_rows(unit):
        return jnp.concatenate([unit[0][unit[1], t] for t in range(TP)], axis=1)

    shared_unit, own_unit = (GS, 0, 0), (GS, 1, 1)
    stages = (Z - 1) * CH
    stage_units = [(GE, n, 2 + n) for n in range(stages)]
    last_unit = (GL, 0, 2 + stages)
    head_units = [(GH, n, 3 + stages + n) for n in range(chunks)]

    tile = min(256, width)

    def hidden(a, gate_w, up_w, unit):
        def turn(n, carry):
            at = pl.ds(pl.multiple_of(n * tile, tile), tile)
            h = silu(dot(a, gate_w[:, at])) * dot(a, up_w[:, at])
            unit[0][unit[1], tp, :, at] = h.astype(bf16)
            return carry

        lax.fori_loop(0, width // tile, turn, 0)

    def send_result(n, h):
        result_sends.start(
            lambda sem: remote(RO.at[n, h], RI.at[ep, h], sem, res_r.at[ep, h], order[n], tp)
        )

    row = lax.broadcasted_iota(jnp.int32, (BLOCK, BLOCK), 0)
    col = lax.broadcasted_iota(jnp.int32, (BLOCK, BLOCK), 1)
    causal = row >= col
    tril = causal.astype(f32)

    def scan_turn(n, _):
        at = pl.ds(pl.multiple_of(n * BLOCK, BLOCK), BLOCK)
        r = r_ref[at, :].astype(f32)
        log_sig = jnp.minimum(r, 0.0) - jnp.log1p(jnp.exp(-jnp.abs(r)))
        rate = log_sig / switch_softness + b_ref[at, :]
        inner = jnp.dot(tril, rate, precision=lax.Precision.HIGHEST, preferred_element_type=f32)
        last = inner[BLOCK - 1 : BLOCK, :]
        q = q_ref[at, :].astype(f32) * DK**-0.5
        k = k_ref[at, :].astype(f32)
        q_in = q * jnp.exp(inner)
        q_b = q_in.astype(bf16)
        k_b = (k * jnp.exp(-inner)).astype(bf16)
        k_out = (k * jnp.exp(last - inner)).astype(bf16)
        prior = state_ref[DV : DV + 1, :]
        far_ref[at, :] = (q * jnp.exp(inner + prior)).astype(bf16)
        entering = state_ref[0:DV, :]
        entering_b = entering.astype(bf16)
        updates = []
        for h in range(heads):
            ks = slice(h * DK, (h + 1) * DK)
            vs = slice(h * DV, (h + 1) * DV)
            v = v_ref[at, vs]
            scores = lax.dot_general(q_b[:, ks], k_b[:, ks], NT, preferred_element_type=f32)
            scores = jnp.where(causal, scores, 0.0).astype(bf16)
            out = jnp.dot(scores, v, preferred_element_type=f32)
            out += lax.dot_general(q_b[:, ks], entering_b[:, ks], NT, preferred_element_type=f32)
            mixed_ref[at, vs] = out
            updates.append(lax.dot_general(v, k_out[:, ks], TN, preferred_element_type=f32))
        state_ref[0:DV, :] = entering * jnp.exp(last) + jnp.concatenate(updates, axis=1)
        state_ref[DV : DV + 1, :] = prior + last
        return 0

    def put_state(dst, n):
        fade = state_ref[DV : DV + 8, :]
        high = fade.astype(bf16)
        low = (fade - high.astype(f32)).astype(bf16)
        dst[n, 0:DV, :] = state_ref[0:DV, :].astype(bf16)
        dst[n, DV : DV + PAD, :] = jnp.concatenate([high, low], axis=0)

    def state_a(dx):
        return remote(A.at[x], A.at[x], a_s.at[dx - 1], a_r.at[dx - 1], z * X + (x + dx) % X, tp)

    def state_b():
        return remote(B.at[0], B.at[1], b_s.at[0], b_r.at[0], (ep + X) % E, tp)

    def fold(src, n, state):
        fade = src[n, DV : DV + PAD, :].astype(f32)
        fade = fade[0:8] + fade[8:16]
        return fade, jnp.exp(fade[0:1]) * state + src[n, 0:DV, :].astype(f32)

    def combine():
        for dx in range(1, X):
            state_a(dx).wait_recv()
        state = jnp.zeros((DV, kw), f32)
        total = jnp.zeros((8, kw), f32)
        for n in range(X):
            fade, state = fold(A, n, state)
            total += fade
        state_ref[0:DV, :] = state
        state_ref[DV : DV + 8, :] = total
        enter_ref[...] = jnp.zeros_like(enter_ref)

    def chain(n):
        @pl.when(z == n)
        def _():
            if n:
                state_b().wait_recv()
                enter_ref[...] = B[1].astype(f32)
            if n < Z - 1:
                through = jnp.exp(state_ref[DV : DV + 1, :]) * enter_ref[...] + state_ref[0:DV, :]
                B[0] = through.astype(bf16)
                state_b().start()

    def enter():
        for n in range(X - 1):
            state = enter_ref[...]
            enter_ref[...] = jnp.where(n < x, fold(A, n, state)[1], state)

    def finish(i):
        at = pl.ds(i * rows, rows)
        state = enter_ref[...].astype(bf16)
        gain = gain_ref[...]
        for h in range(heads):
            ks = slice(h * DK, (h + 1) * DK)
            vs = slice(h * DV, (h + 1) * DV)
            m = mixed_ref[at, vs] + lax.dot_general(
                far_ref[at, ks], state[:, ks], NT, preferred_element_type=f32
            )
            scale = lax.rsqrt(jnp.mean(m * m, axis=-1, keepdims=True) + eps_norm)
            gate = silu(og_ref[at, vs].astype(f32))
            GH[i, tp, :, vs] = (m * scale * gain * gate).astype(bf16)

    order = [z * X + (x + dx) % X for dx in range(X)]
    for j in range(1, Z):
        order += [near(j) * X + (x + dx) % X for dx in range(X)]

    def expert_hidden(pieces, unit):
        for n, h in pieces:
            row_part(order[n], h).wait_recv()
        a = jnp.concatenate([rows_of(order[n], h) for n, h in pieces], axis=0)
        hidden(a, eg_ref, eu_ref, unit)
        unit_send(unit)

    def expert_result(pieces, unit, hold=None):
        unit_wait(unit)
        out = dot(unit_rows(unit), ed_ref[...]).astype(bf16)
        size = part * CORES
        for i, (n, h) in enumerate(pieces):
            RO[n, h] = out[i * size : (i + 1) * size]
        for n, h in pieces:
            if n % X and hold is not None:
                hold.append((n, h))
            elif n:
                send_result(n, h)

    turns = seq // BLOCK
    ahead = 1

    def scan(lo, hi):
        lax.fori_loop(lo, hi, scan_turn, 0, unroll=2)

    for h in range(CH):
        send_own(h)
    own = jnp.concatenate([rows_of(ep, h) for h in range(CH)], axis=0)
    need(sg_ref, su_ref)
    hidden(own, sg_ref, su_ref, shared_unit)
    unit_send(shared_unit)
    need(eg_ref, eu_ref)
    hidden(own, eg_ref, eu_ref, own_unit)
    unit_send(own_unit)
    need(r_ref, b_ref, q_ref, k_ref, v_ref)
    load(late)
    state_ref[...] = jnp.zeros_like(state_ref)
    own_pieces = [(0, h) for h in range(CH)]
    stage_pieces = []

    def states():
        put_state(A, x)
        for dx in range(1, X):
            state_a(dx).start()

    def shared_down():
        need(sd_ref)
        unit_wait(shared_unit)
        acc_ref[...] = dot(unit_rows(shared_unit), sd_ref[...])
        need(ed_ref)
        expert_result(own_pieces, own_unit)

    def forward(unit):
        unit_forward(unit)

    def mixing(what):
        if what == 0:
            combine()
        chain(what)

    scan(0, turns // 2)
    fillers = {
        0: lambda: scan(turns // 2, 3 * turns // 4),
        1: lambda: (scan(3 * turns // 4, turns), states()),
    }
    held = []
    for n in range(stages):
        j, h = n // CH + 1, n % CH
        relay_line(j, h)
        for dx in range(1, X):
            relay_side(j - 1, h, dx)
        if n > stages - Z:
            mixing(n - (stages - Z) - 1)
        stage_pieces.append([((j - 1) * X + dx, h) for dx in range(1, X)] + [(j * X, h)])
        fillers.get(n, lambda: None)()
        if n >= 3:
            expert_result(stage_pieces[n - 3], stage_units[n - 3], held)
        if n == 1:
            forward(shared_unit)
            forward(own_unit)
        if n == 2:
            shared_down()
        expert_hidden(stage_pieces[n], stage_units[n])
        if n >= 2:
            forward(stage_units[n - 2])
    mixing(Z - 1)
    need(og_ref, gain_ref)
    enter()
    for i in range(chunks):
        finish(i)
        if i < ahead:
            unit_send(head_units[i])
    forward(stage_units[-2])
    for n in (stages - 3, stages - 2):
        expert_result(stage_pieces[n], stage_units[n], held)
    last_pieces = [((Z - 1) * X + dx, h) for dx in range(1, X) for h in range(CH)]
    for h in range(CH):
        for dx in range(1, X):
            relay_side(Z - 1, h, dx)
    for piece in held:
        send_result(*piece)
    expert_hidden(last_pieces, last_unit)
    for unit in head_units[ahead:]:
        unit_send(unit)
    forward(stage_units[-1])
    expert_result(stage_pieces[-1], stage_units[-1])
    need(wo_ref)
    need(idx_ref, w_ref)

    index, given = idx_ref[...], w_ref[...]
    by_expert = [jnp.sum(jnp.where(index == e, given, 0.0), axis=0, keepdims=True) for e in range(E)]
    by_expert = jnp.transpose(jnp.concatenate(by_expert, axis=0), (1, 0))
    lane = lax.broadcasted_iota(jnp.int32, by_expert.shape, 1)

    def weight(e):
        return jnp.sum(jnp.where(lane == e, by_expert, 0.0), axis=1, keepdims=True)

    def mixer_out(i):
        at = pl.ds(i * rows, rows)
        return pltpu.make_async_copy(mixer_ref.at[at], mixer_hbm.at[at], out_sem.at[i])

    def mixer(i):
        unit_wait(head_units[i])
        at = pl.ds(i * rows, rows)
        mixer_ref[at, :] = dot(unit_rows(head_units[i]), wo_ref[...]).astype(bf16)
        mixer_out(i).start()

    def add(e, got):
        full = jnp.concatenate([got(h) for h in range(CH)], axis=0)
        acc_ref[...] += full.astype(f32) * weight(e)

    def collect(ns):
        for n in ns:
            e = order[n]
            for h in range(CH):
                remote(RO.at[n, h], RI.at[e, h], res_s.at[0], res_r.at[e, h], e, tp).wait_recv()
            add(e, lambda h: RI[e, h])

    for i in range(ahead):
        forward(head_units[i])
    forward(last_unit)
    for i in range(ahead):
        mixer(i)
    expert_result(last_pieces, last_unit)
    add(ep, lambda h: RO[0, h])
    for i in range(ahead, chunks):
        forward(head_units[i])
        mixer(i)
    collect(range(1, E))
    blend_ref[...] = acc_ref[...].astype(bf16)
    blend_out = pltpu.make_async_copy(blend_ref, blend_hbm, out_sem.at[chunks])
    blend_out.start()

    for h in range(CH):
        pl.when(z < Z - 1)(lambda: row_up(ep, h).wait_send())
        pl.when(z > 0)(lambda: row_down(ep, h, r_down_s.at[h]).wait_send())
        for k in range(1, Z):
            pl.when((z >= k) & (z < Z - 1))(lambda: row_up(ep - k * X, h).wait_send())
            pl.when((z + k < Z) & (z > 0))(lambda: row_down(ep + k * X, h).wait_send())
        for k in range(Z):
            for dx in range(1, X):
                row_x(near(k) * X + x, h, dx).wait_send()
        pl.when(z > 0)(lambda: row_part(ep, h, 0).wait_send())
        pl.when(z < Z - 1)(lambda: row_part(ep, h, 1).wait_send())
        for dx in range(1, X):
            row_part(ep, h, 1 + dx).wait_send()
    for sends in (part_sends, *y_sends, *f_sends, result_sends):
        sends.drain()
    for dx in range(1, X):
        state_a(dx).wait_send()
    pl.when(z < Z - 1)(lambda: state_b().wait_send())
    for i in range(chunks):
        mixer_out(i).wait()
    blend_out.wait()


def local(
    queries,
    sequence_keys,
    stream_content_vectors,
    output_gate_logits,
    retention_preactivation,
    additional_fade_bias,
    attention_group_rescale,
    output_projection,
    expert_batch_tokens,
    expert_norm_gain,
    routed_expert_index,
    routed_expert_weights,
    expert_gate_matrix,
    expert_up_matrix,
    expert_down_matrix,
    shared_gate_matrix,
    shared_up_matrix,
    shared_down_matrix,
):
    experts, lanes = lax.axis_size("ep"), lax.axis_size("tp")
    X = 2 ** (int(math.log2(experts)) // 2)
    Z, Y = experts // X, lanes // CORES
    rows, model_width = expert_batch_tokens.shape
    seq, kw = queries.shape
    vw = stream_content_vectors.shape[1]
    width = shared_gate_matrix.shape[1]
    chunks = seq // rows
    stages = (Z - 1) * CH
    units = 3 + stages + chunks
    args = (
        queries,
        sequence_keys,
        stream_content_vectors,
        output_gate_logits,
        retention_preactivation,
        additional_fade_bias,
        attention_group_rescale.reshape(1, DV),
        output_projection,
        expert_batch_tokens,
        expert_norm_gain.reshape(1, model_width),
        routed_expert_index.T,
        routed_expert_weights.T,
        expert_gate_matrix[0],
        expert_up_matrix[0],
        expert_down_matrix[0],
        shared_gate_matrix,
        shared_up_matrix,
        shared_down_matrix,
    )
    outs = (
        jax.ShapeDtypeStruct((seq, output_projection.shape[1]), bf16),
        jax.ShapeDtypeStruct((rows, shared_down_matrix.shape[1]), bf16),
    )
    dma = lambda *shape: pltpu.SemaphoreType.DMA(shape)
    scratch = [pltpu.VMEM(a.shape, a.dtype) for a in args]
    scratch += [pltpu.VMEM(o.shape, o.dtype) for o in outs]
    scratch += [
        pltpu.VMEM((experts, CH, CORES, rows // (CH * CORES), model_width), bf16),
        pltpu.VMEM((2, lanes, rows, width), bf16),
        pltpu.VMEM((stages, lanes, X * rows // CH, width), bf16),
        pltpu.VMEM((1, lanes, (X - 1) * rows, width), bf16),
        pltpu.VMEM((chunks, lanes, rows, vw), bf16),
        pltpu.VMEM((experts, CH, rows // CH, outs[1].shape[1]), bf16),
        pltpu.VMEM((experts, CH, rows // CH, outs[1].shape[1]), bf16),
        pltpu.VMEM((X, DV + PAD, kw), bf16),
        pltpu.VMEM((2, DV, kw), bf16),
        pltpu.VMEM((seq, vw), f32),
        pltpu.VMEM((seq, kw), bf16),
        pltpu.VMEM((DV + 8, kw), f32),
        pltpu.VMEM((DV, kw), f32),
        pltpu.VMEM((rows, outs[1].shape[1]), f32),
        dma(11),
        dma(chunks + 1),
        dma(1 + X, CH),
        dma(Z, CH),
        dma(CH),
        dma(X - 1, Z, CH),
        dma(experts, CH),
        dma(experts, CH),
        dma(5),
        dma(units),
        dma(Y - 1, 9),
        dma(Y - 1, units),
        dma(Y - 1, 3),
        dma(Y - 1, units),
        dma(14),
        dma(experts, CH),
        dma(X - 1),
        dma(X - 1),
        dma(1),
        dma(1),
    ]
    made = pl.pallas_call(
        functools.partial(body, (Z, X, Y)),
        out_shape=outs,
        in_specs=[pl.BlockSpec(memory_space=pl.ANY)] * len(args),
        out_specs=tuple([pl.BlockSpec(memory_space=pl.ANY)] * len(outs)),
        scratch_shapes=scratch,
        compiler_params=pltpu.CompilerParams(
            collective_id=0, has_side_effects=True, vmem_limit_bytes=66000000
        ),
        cost_estimate=pl.CostEstimate(
            flops=10**10, bytes_accessed=20 * 2**20, transcendentals=10**6
        ),
        name="step",
    )(*args)
    return pl.pallas_call(
        settle,
        out_shape=outs,
        in_specs=[pl.BlockSpec(memory_space=pl.ANY)] * 2,
        out_specs=tuple([pl.BlockSpec(memory_space=pl.ANY)] * 2),
        scratch_shapes=[pltpu.VMEM(o.shape, o.dtype) for o in outs] + [dma(4)],
        cost_estimate=pl.CostEstimate(flops=10**6, bytes_accessed=2**21, transcendentals=0),
        name="settle",
    )(*made)


def settle(mixer_in, blend_in, mixer_out, blend_out, mixer_ref, blend_ref, sem):
    reads = [
        pltpu.make_async_copy(mixer_in, mixer_ref, sem.at[0]),
        pltpu.make_async_copy(blend_in, blend_ref, sem.at[1]),
    ]
    writes = [
        pltpu.make_async_copy(mixer_ref, mixer_out, sem.at[2]),
        pltpu.make_async_copy(blend_ref, blend_out, sem.at[3]),
    ]
    for copy in reads:
        copy.start()
    for read, write in zip(reads, writes):
        read.wait()
        write.start()
    for copy in writes:
        copy.wait()


def solution(mesh):
    in_specs = (
        P("ep", "tp"),
        P("ep", "tp"),
        P("ep", "tp"),
        P("ep", "tp"),
        P("ep", "tp"),
        P("ep", "tp"),
        P(),
        P(None, "tp"),
        P("ep", None),
        P(),
        P("ep", None),
        P("ep", None),
        P("ep", None, "tp"),
        P("ep", None, "tp"),
        P("ep", None, "tp"),
        P(None, "tp"),
        P(None, "tp"),
        P(None, "tp"),
    )
    out_specs = (P("ep", "tp"), P("ep", "tp"))
    return jax.shard_map(local, mesh=mesh, in_specs=in_specs, out_specs=out_specs, check_vma=False)
```

profile of v0, /device:TPU:0, one launch (start us, length us, event | category | flops | bytes accessed | tf_op | source)
XLA Modules:
  0.0 55.1 jit_solution(2646047533256983381)
XLA Ops:
  0.6 52.4 %step.1 = (bf16[512,512]{1,0:T(8,128)(2,1)}, bf16[128,512]{1,0:T(8,128)(2,1)}) custom-call(bf16[512,256]{1,0:T(8,128)(2,1)} %refs_0_.1, bf16[512,256]{1,0:T(8,128)(2,1)} %refs_1_.1, bf16[512,512]{1,0:T(8,128)(2,1)} %refs_2_.1, bf16[512,512]{1,0:T(8,128)(2,1)} %refs_3_.1, bf16[512,256]{1,0:T(8,128)(2,1)} %refs_4_.1, f32[512,256]{1,0:T(8,128)} %refs_5_.1, ...), custom_call_target="tpu_custom_call" | custom-call | flops 10000000000 | bytes 20971520 | tf_op jit(solution)/shard_map/step/pallas_call | solution.py:626
  53.1 1.9 %settle.1 = (bf16[512,512]{1,0:T(8,128)(2,1)}, bf16[128,512]{1,0:T(8,128)(2,1)}) custom-call(bf16[512,512]{1,0:T(8,128)(2,1)} %get-tuple-element.4.mixer_in, bf16[128,512]{1,0:T(8,128)(2,1)} %get-tuple-element.5.blend_in), custom_call_target="tpu_custom_call" | custom-call | flops 1000000 | bytes 2097152 | tf_op jit(solution)/shard_map/settle/pallas_call | solution.py:640
where the time goes:
time: 55.3 us; the launch traced here: 55.1 us
  Pallas kernels  54.3 us (98%)
  between operations  0.81 us (1%)
    pallas_call x1, Pallas kernels, local(): pl.pallas_call(functools.partial(body, (Z, X, Y)), out_shape=outs, in_spe...  52.4 us
    pallas_call x1, Pallas kernels, local(): pl.pallas_call(settle, out_shape=outs, in_specs=[pl.BlockSpec(memory_spac...  1.9 us

commit v1 on v0

--- a/solution.py
+++ b/solution.py
@@ -38,13 +38,12 @@
     (
         q_hbm, k_hbm, v_hbm, og_hbm, r_hbm, b_hbm, gain_hbm, wo_hbm, tok_hbm, ng_hbm, idx_hbm, w_hbm,
         eg_hbm, eu_hbm, ed_hbm, sg_hbm, su_hbm, sd_hbm,
-        mixer_hbm, blend_hbm,
+        mixer_ref, blend_ref,
         q_ref, k_ref, v_ref, og_ref, r_ref, b_ref, gain_ref, wo_ref, tok_ref, ng_ref, idx_ref, w_ref,
         eg_ref, eu_ref, ed_ref, sg_ref, su_ref, sd_ref,
-        mixer_ref, blend_ref,
         R, GS, GE, GL, GH, RO, RI, A, B, mixed_ref, far_ref, state_ref, enter_ref, acc_ref,
-        in_sem, out_sem,
-        r_part_s, r_z_s, r_down_s, r_x_s, r_far_r, r_part_r,
+        in_sem,
+        r_part_s, r_z_s, r_down_s, r_x_s, r_side_s, r_far_r, r_part_r,
         u_part_s, u_part_r, u_y_s, u_y_r, u_f_s, u_f_r,
         res_s, res_r, a_s, a_r, b_s, b_r,
     ) = refs
@@ -180,13 +179,52 @@
             pl.when(z > 0)(lambda: row_down(b, h).start())
             hand_over(b, h, 1, k > 1)
 
-        for dx in range(1, X):
-            row_x(near(k) * X + x, h, dx).start()
+        @pl.when(inner(near(k)))
+        def _():
+            for dx in range(1, X):
+                row_x(near(k) * X + x, h, dx).start()
+
+    def inner(zj):
+        return (zj > 0) & (zj < Z - 1)
+
+    def side(j, dx):
+        return near(j) * X + (x + dx) % X
+
+    def top(dx):
+        return (Z - 1) * X + (x + dx) % X
+
+    def bottom(dx):
+        return (x + dx) % X
+
+    def side_row(b, h, up, dx):
+        there = ep + X if up else ep - X
+        sem = r_side_s.at[dx - 1, int(up), h]
+        return remote(R.at[b, h, c], R.at[b, h, c], sem, r_far_r.at[b, h], there, tp)
 
     def relay_side(j, h, dx):
-        b = near(j) * X + (x + dx) % X
-        arrive(b, h)
-        hand_over(b, h, 1 + dx, j > 0)
+        kind = 2 + (dx - 1) * (Z + 2)
+
+        def here(b, n):
+            arrive(b, h)
+            row_part(b, h, kind + n).start()
+
+        if j == 0:
+            here(side(0, dx), 0)
+            pl.when(z == 0)(lambda: side_row(bottom(dx), h, True, dx).start())
+            pl.when(z == Z - 1)(lambda: side_row(top(dx), h, False, dx).start())
+            return
+
+        pl.when(inner(near(j)))(lambda: here(side(j, dx), j))
+
+        @pl.when(z == Z - 1 - j)
+        def _():
+            here(top(dx), Z)
+            pl.when(z > 0)(lambda: side_row(top(dx), h, False, dx).start())
+
+        @pl.when(z == j)
+        def _():
+            here(bottom(dx), Z + 1)
+            pl.when(z < Z - 1)(lambda: side_row(bottom(dx), h, True, dx).start())
 
     def rows_of(b, h):
         return jnp.concatenate([R[b, h, n] for n in range(CORES)], axis=0)
@@ -374,7 +412,6 @@
                 send_result(n, h)
 
     turns = seq // BLOCK
-    ahead = 1
 
     def scan(lo, hi):
         lax.fori_loop(lo, hi, scan_turn, 0, unroll=2)
@@ -425,10 +462,12 @@
         relay_line(j, h)
         for dx in range(1, X):
             relay_side(j - 1, h, dx)
-        if n > stages - Z:
-            mixing(n - (stages - Z) - 1)
         stage_pieces.append([((j - 1) * X + dx, h) for dx in range(1, X)] + [(j * X, h)])
         fillers.get(n, lambda: None)()
+        if n == stages - 1:
+            for piece in held:
+                send_result(*piece)
+            held = None
         if n >= 3:
             expert_result(stage_pieces[n - 3], stage_units[n - 3], held)
         if n == 1:
@@ -437,27 +476,29 @@
         if n == 2:
             shared_down()
         expert_hidden(stage_pieces[n], stage_units[n])
+        if n > stages - Z:
+            mixing(n - (stages - Z) - 1)
         if n >= 2:
             forward(stage_units[n - 2])
-    mixing(Z - 1)
-    need(og_ref, gain_ref)
-    enter()
-    for i in range(chunks):
-        finish(i)
-        if i < ahead:
-            unit_send(head_units[i])
-    forward(stage_units[-2])
-    for n in (stages - 3, stages - 2):
-        expert_result(stage_pieces[n], stage_units[n], held)
     last_pieces = [((Z - 1) * X + dx, h) for dx in range(1, X) for h in range(CH)]
     for h in range(CH):
         for dx in range(1, X):
             relay_side(Z - 1, h, dx)
-    for piece in held:
+    for piece in held or ():
         send_result(*piece)
+    expert_result(stage_pieces[stages - 3], stage_units[stages - 3])
     expert_hidden(last_pieces, last_unit)
-    for unit in head_units[ahead:]:
-        unit_send(unit)
+    forward(stage_units[-2])
+    mixing(Z - 1)
+    need(og_ref, gain_ref)
+    enter()
+    for i in range(chunks // 2):
+        finish(i)
+        unit_send(head_units[i])
+    expert_result(stage_pieces[-2], stage_units[-2])
+    for i in range(chunks // 2, chunks):
+        finish(i)
+        unit_send(head_units[i])
     forward(stage_units[-1])
     expert_result(stage_pieces[-1], stage_units[-1])
     need(wo_ref)
@@ -471,15 +512,10 @@
     def weight(e):
         return jnp.sum(jnp.where(lane == e, by_expert, 0.0), axis=1, keepdims=True)
 
-    def mixer_out(i):
-        at = pl.ds(i * rows, rows)
-        return pltpu.make_async_copy(mixer_ref.at[at], mixer_hbm.at[at], out_sem.at[i])
-
     def mixer(i):
         unit_wait(head_units[i])
         at = pl.ds(i * rows, rows)
         mixer_ref[at, :] = dot(unit_rows(head_units[i]), wo_ref[...]).astype(bf16)
-        mixer_out(i).start()
 
     def add(e, got):
         full = jnp.concatenate([got(h) for h in range(CH)], axis=0)
@@ -492,20 +528,14 @@
                 remote(RO.at[n, h], RI.at[e, h], res_s.at[0], res_r.at[e, h], e, tp).wait_recv()
             add(e, lambda h: RI[e, h])
 
-    for i in range(ahead):
-        forward(head_units[i])
     forward(last_unit)
-    for i in range(ahead):
-        mixer(i)
     expert_result(last_pieces, last_unit)
     add(ep, lambda h: RO[0, h])
-    for i in range(ahead, chunks):
+    for i in range(chunks):
         forward(head_units[i])
         mixer(i)
     collect(range(1, E))
     blend_ref[...] = acc_ref[...].astype(bf16)
-    blend_out = pltpu.make_async_copy(blend_ref, blend_hbm, out_sem.at[chunks])
-    blend_out.start()
 
     for h in range(CH):
         pl.when(z < Z - 1)(lambda: row_up(ep, h).wait_send())
@@ -513,21 +543,24 @@
         for k in range(1, Z):
             pl.when((z >= k) & (z < Z - 1))(lambda: row_up(ep - k * X, h).wait_send())
             pl.when((z + k < Z) & (z > 0))(lambda: row_down(ep + k * X, h).wait_send())
-        for k in range(Z):
-            for dx in range(1, X):
-                row_x(near(k) * X + x, h, dx).wait_send()
+        for dx in range(1, X):
+            kind = 2 + (dx - 1) * (Z + 2)
+            row_x(ep, h, dx).wait_send()
+            row_part(ep, h, kind).wait_send()
+            for k in range(1, Z):
+                pl.when(inner(near(k)))(lambda: row_x(near(k) * X + x, h, dx).wait_send())
+                pl.when(inner(near(k)))(lambda: row_part(ep, h, kind + k).wait_send())
+            pl.when(z < Z - 1)(lambda: row_part(ep, h, kind + Z).wait_send())
+            pl.when(z > 0)(lambda: row_part(ep, h, kind + Z + 1).wait_send())
+            pl.when(z < Z - 1)(lambda: side_row(ep, h, True, dx).wait_send())
+            pl.when(z > 0)(lambda: side_row(ep, h, False, dx).wait_send())
         pl.when(z > 0)(lambda: row_part(ep, h, 0).wait_send())
         pl.when(z < Z - 1)(lambda: row_part(ep, h, 1).wait_send())
-        for dx in range(1, X):
-            row_part(ep, h, 1 + dx).wait_send()
     for sends in (part_sends, *y_sends, *f_sends, result_sends):
         sends.drain()
     for dx in range(1, X):
         state_a(dx).wait_send()
     pl.when(z < Z - 1)(lambda: state_b().wait_send())
-    for i in range(chunks):
-        mixer_out(i).wait()
-    blend_out.wait()
 
 
 def local(
@@ -586,7 +619,6 @@
     )
     dma = lambda *shape: pltpu.SemaphoreType.DMA(shape)
     scratch = [pltpu.VMEM(a.shape, a.dtype) for a in args]
-    scratch += [pltpu.VMEM(o.shape, o.dtype) for o in outs]
     scratch += [
         pltpu.VMEM((experts, CH, CORES, rows // (CH * CORES), model_width), bf16),
         pltpu.VMEM((2, lanes, rows, width), bf16),
@@ -603,11 +635,11 @@
         pltpu.VMEM((DV, kw), f32),
         pltpu.VMEM((rows, outs[1].shape[1]), f32),
         dma(11),
-        dma(chunks + 1),
-        dma(1 + X, CH),
+        dma(2 + (X - 1) * (Z + 2), CH),
         dma(Z, CH),
         dma(CH),
         dma(X - 1, Z, CH),
+        dma(X - 1, 2, CH),
         dma(experts, CH),
         dma(experts, CH),
         dma(5),
@@ -625,9 +657,9 @@
     ]
     made = pl.pallas_call(
         functools.partial(body, (Z, X, Y)),
-        out_shape=outs,
+        out_shape=tuple(pltpu.VMEM(o.shape, o.dtype) for o in outs),
         in_specs=[pl.BlockSpec(memory_space=pl.ANY)] * len(args),
-        out_specs=tuple([pl.BlockSpec(memory_space=pl.ANY)] * len(outs)),
+        out_specs=tuple([pl.BlockSpec(memory_space=pltpu.VMEM)] * len(outs)),
         scratch_shapes=scratch,
         compiler_params=pltpu.CompilerParams(
             collective_id=0, has_side_effects=True, vmem_limit_bytes=66000000
@@ -640,28 +672,21 @@
     return pl.pallas_call(
         settle,
         out_shape=outs,
-        in_specs=[pl.BlockSpec(memory_space=pl.ANY)] * 2,
+        in_specs=[pl.BlockSpec(memory_space=pltpu.VMEM)] * 2,
         out_specs=tuple([pl.BlockSpec(memory_space=pl.ANY)] * 2),
-        scratch_shapes=[pltpu.VMEM(o.shape, o.dtype) for o in outs] + [dma(4)],
+        scratch_shapes=[dma(2)],
         cost_estimate=pl.CostEstimate(flops=10**6, bytes_accessed=2**21, transcendentals=0),
         name="settle",
-    )(*made)
-
-
-def settle(mixer_in, blend_in, mixer_out, blend_out, mixer_ref, blend_ref, sem):
-    reads = [
-        pltpu.make_async_copy(mixer_in, mixer_ref, sem.at[0]),
-        pltpu.make_async_copy(blend_in, blend_ref, sem.at[1]),
+    )(*[pltpu.with_memory_space_constraint(m, pltpu.VMEM) for m in made])
+
+
+def settle(mixer_ref, blend_ref, mixer_out, blend_out, sem):
+    writes = [
+        pltpu.make_async_copy(mixer_ref, mixer_out, sem.at[0]),
+        pltpu.make_async_copy(blend_ref, blend_out, sem.at[1]),
     ]
-    writes = [
-        pltpu.make_async_copy(mixer_ref, mixer_out, sem.at[2]),
-        pltpu.make_async_copy(blend_ref, blend_out, sem.at[3]),
-    ]
-    for copy in reads:
+    for copy in writes:
         copy.start()
-    for read, write in zip(reads, writes):
-        read.wait()
-        write.start()
     for copy in writes:
         copy.wait()
 

time: 55.3 us -> 53.8 us (0.973)
  Pallas kernels: 54.3 us -> 52.8 us
    pallas_call x1, Pallas kernels: 1.9 us -> 0.85 us  [local(): pl.pallas_call(settle, out_shape=outs, in_specs=[pl.BlockSpec(memory_spac...]
where the time goes in v1:
time: 53.8 us; the launch traced here: 53.7 us
  Pallas kernels  52.8 us (98%)
  between operations  0.81 us (2%)
    pallas_call x1, Pallas kernels, local(): pl.pallas_call(functools.partial(body, (Z, X, Y)), out_shape=tuple((pltpu...  52 us

profile of v1, /device:TPU:0, one launch (start us, length us, event | category | flops | bytes accessed | tf_op | source)
XLA Modules:
  0.0 53.7 jit_solution(7443507536578506991)
XLA Ops:
  0.6 52.0 %step.1 = (bf16[512,512]{1,0:T(8,128)(2,1)S(1)}, bf16[128,512]{1,0:T(8,128)(2,1)S(1)}) custom-call(bf16[512,256]{1,0:T(8,128)(2,1)} %refs_0_.1, bf16[512,256]{1,0:T(8,128)(2,1)} %refs_1_.1, bf16[512,512]{1,0:T(8,128)(2,1)} %refs_2_.1, bf16[512,512]{1,0:T(8,128)(2,1)} %refs_3_.1, bf16[512,256]{1,0:T(8,128)(2,1)} %refs_4_.1, f32[512,256]{1,0:T(8,128)} %refs_5_.1, ...), custom_call_target="tpu_custom_call" | custom-call | flops 10000000000 | bytes 20971520 | tf_op jit(solution)/shard_map/step/pallas_call | solution.py:658
  52.6 0.8 %settle.1 = (bf16[512,512]{1,0:T(8,128)(2,1)}, bf16[128,512]{1,0:T(8,128)(2,1)}) custom-call(bf16[512,512]{1,0:T(8,128)(2,1)S(1)} %get-tuple-element.4.mixer_ref, bf16[128,512]{1,0:T(8,128)(2,1)S(1)} %get-tuple-element.5.blend_ref), custom_call_target="tpu_custom_call" | custom-call | flops 1000000 | bytes 2097152 | tf_op jit(solution)/shard_map/settle/pallas_call | solution.py:672

commit v2 on v1

--- a/solution.py
+++ b/solution.py
@@ -34,7 +34,7 @@
 
 def body(sizes, *refs):
     Z, X, Y = sizes
-    E, TP = Z * X, Y * CORES
+    E = Z * X
     (
         q_hbm, k_hbm, v_hbm, og_hbm, r_hbm, b_hbm, gain_hbm, wo_hbm, tok_hbm, ng_hbm, idx_hbm, w_hbm,
         eg_hbm, eu_hbm, ed_hbm, sg_hbm, su_hbm, sd_hbm,
@@ -56,7 +56,8 @@
     seq, kw = q_ref.shape
     heads = kw // DK
     chunks = seq // rows
-    width = GS.shape[-1]
+    tiles, tile = GS.shape[2], GS.shape[-1]
+    width = tiles * tile
     part = rows // (CH * CORES)
 
     def remote(src, dst, ssem, rsem, e, t):
@@ -179,13 +180,19 @@
             pl.when(z > 0)(lambda: row_down(b, h).start())
             hand_over(b, h, 1, k > 1)
 
-        @pl.when(inner(near(k)))
+        @pl.when(by_x(near(k), h))
         def _():
             for dx in range(1, X):
                 row_x(near(k) * X + x, h, dx).start()
 
-    def inner(zj):
-        return (zj > 0) & (zj < Z - 1)
+    def by_x(zj, h):
+        use = (zj > 0) & (zj < Z - 1)
+        if h == CH - 1:
+            use |= (zj + z == Z - 1) & ((z == 0) | (z == Z - 1))
+        return use
+
+    def spare(h):
+        return 1 if h == CH - 1 else 0
 
     def side(j, dx):
         return near(j) * X + (x + dx) % X
@@ -214,17 +221,17 @@
             pl.when(z == Z - 1)(lambda: side_row(top(dx), h, False, dx).start())
             return
 
-        pl.when(inner(near(j)))(lambda: here(side(j, dx), j))
+        pl.when((near(j) > 0) & (near(j) < Z - 1))(lambda: here(side(j, dx), j))
 
         @pl.when(z == Z - 1 - j)
         def _():
             here(top(dx), Z)
-            pl.when(z > 0)(lambda: side_row(top(dx), h, False, dx).start())
+            pl.when(z > spare(h))(lambda: side_row(top(dx), h, False, dx).start())
 
         @pl.when(z == j)
         def _():
             here(bottom(dx), Z + 1)
-            pl.when(z < Z - 1)(lambda: side_row(bottom(dx), h, True, dx).start())
+            pl.when(z < Z - 1 - spare(h))(lambda: side_row(bottom(dx), h, True, dx).start())
 
     def rows_of(b, h):
         return jnp.concatenate([R[b, h, n] for n in range(CORES)], axis=0)
@@ -239,11 +246,11 @@
         sem = u_part_s.at[0] if sem is None else sem
         return remote(G.at[n, tp], G.at[n, tp], sem, u_part_r.at[u], ep, partner)
 
-    def unit_y(unit, dy, sem=None):
+    def unit_y(unit, dy, m, sem=None):
         G, n, u = unit
         t = (y + dy) % Y * CORES + c
         sem = u_y_s.at[dy - 1, 0] if sem is None else sem
-        return remote(G.at[n, tp], G.at[n, tp], sem, u_y_r.at[dy - 1, u], ep, t)
+        return remote(G.at[n, tp, m], G.at[n, tp, m], sem, u_y_r.at[dy - 1, u, m], ep, t)
 
     def unit_f(unit, dy, sem=None):
         G, n, u = unit
@@ -251,23 +258,36 @@
         sem = u_f_s.at[dy - 1, 0] if sem is None else sem
         return remote(G.at[n, t], G.at[n, t], sem, u_f_r.at[dy - 1, u], ep, partner)
 
+    def unit_send_tile(unit, m):
+        for dy in range(1, Y):
+            y_sends[dy - 1].start(lambda sem: unit_y(unit, dy, m, sem))
+        if m == tiles - 1:
+            part_sends.start(lambda sem: unit_part(unit, sem))
+
     def unit_send(unit):
-        for dy in range(1, Y):
-            y_sends[dy - 1].start(lambda sem: unit_y(unit, dy, sem))
-        part_sends.start(lambda sem: unit_part(unit, sem))
+        for m in range(tiles):
+            unit_send_tile(unit, m)
 
     def unit_forward(unit):
         for dy in range(1, Y):
-            unit_y(unit, dy).wait_recv()
+            for m in range(tiles):
+                unit_y(unit, dy, m).wait_recv()
             f_sends[dy - 1].start(lambda sem: unit_f(unit, dy, sem))
 
-    def unit_wait(unit):
+    def unit_dot(unit, w_ref):
+        G, n = unit[:2]
+
+        def pieces(ts):
+            a = [G[n, t, m] for t in ts for m in range(tiles)]
+            w = [w_ref[pl.ds(pl.multiple_of(t * width, width), width), :] for t in ts]
+            return dot(jnp.concatenate(a, axis=1), jnp.concatenate(w, axis=0))
+
         unit_part(unit).wait_recv()
+        chips = [(y - dy + Y) % Y for dy in range(1, Y)]
+        out = pieces([tp, partner, *(chip * CORES + c for chip in chips)])
         for dy in range(1, Y):
             unit_f(unit, dy).wait_recv()
-
-    def unit_rows(unit):
-        return jnp.concatenate([unit[0][unit[1], t] for t in range(TP)], axis=1)
+        return out + pieces([chip * CORES + 1 - c for chip in chips])
 
     shared_unit, own_unit = (GS, 0, 0), (GS, 1, 1)
     stages = (Z - 1) * CH
@@ -275,16 +295,12 @@
     last_unit = (GL, 0, 2 + stages)
     head_units = [(GH, n, 3 + stages + n) for n in range(chunks)]
 
-    tile = min(256, width)
-
     def hidden(a, gate_w, up_w, unit):
-        def turn(n, carry):
-            at = pl.ds(pl.multiple_of(n * tile, tile), tile)
+        for m in range(tiles):
+            at = slice(m * tile, (m + 1) * tile)
             h = silu(dot(a, gate_w[:, at])) * dot(a, up_w[:, at])
-            unit[0][unit[1], tp, :, at] = h.astype(bf16)
-            return carry
-
-        lax.fori_loop(0, width // tile, turn, 0)
+            unit[0][unit[1], tp, m] = h.astype(bf16)
+            unit_send_tile(unit, m)
 
     def send_result(n, h):
         result_sends.start(
@@ -386,7 +402,8 @@
             )
             scale = lax.rsqrt(jnp.mean(m * m, axis=-1, keepdims=True) + eps_norm)
             gate = silu(og_ref[at, vs].astype(f32))
-            GH[i, tp, :, vs] = (m * scale * gain * gate).astype(bf16)
+            at_tile = slice(h * DV % tile, h * DV % tile + DV)
+            GH[i, tp, h * DV // tile, :, at_tile] = (m * scale * gain * gate).astype(bf16)
 
     order = [z * X + (x + dx) % X for dx in range(X)]
     for j in range(1, Z):
@@ -397,11 +414,9 @@
             row_part(order[n], h).wait_recv()
         a = jnp.concatenate([rows_of(order[n], h) for n, h in pieces], axis=0)
         hidden(a, eg_ref, eu_ref, unit)
-        unit_send(unit)
 
     def expert_result(pieces, unit, hold=None):
-        unit_wait(unit)
-        out = dot(unit_rows(unit), ed_ref[...]).astype(bf16)
+        out = unit_dot(unit, ed_ref).astype(bf16)
         size = part * CORES
         for i, (n, h) in enumerate(pieces):
             RO[n, h] = out[i * size : (i + 1) * size]
@@ -414,17 +429,15 @@
     turns = seq // BLOCK
 
     def scan(lo, hi):
-        lax.fori_loop(lo, hi, scan_turn, 0, unroll=2)
+        lax.fori_loop(lo, hi, scan_turn, 0, unroll=hi - lo)
 
     for h in range(CH):
         send_own(h)
     own = jnp.concatenate([rows_of(ep, h) for h in range(CH)], axis=0)
     need(sg_ref, su_ref)
     hidden(own, sg_ref, su_ref, shared_unit)
-    unit_send(shared_unit)
     need(eg_ref, eu_ref)
     hidden(own, eg_ref, eu_ref, own_unit)
-    unit_send(own_unit)
     need(r_ref, b_ref, q_ref, k_ref, v_ref)
     load(late)
     state_ref[...] = jnp.zeros_like(state_ref)
@@ -438,8 +451,7 @@
 
     def shared_down():
         need(sd_ref)
-        unit_wait(shared_unit)
-        acc_ref[...] = dot(unit_rows(shared_unit), sd_ref[...])
+        acc_ref[...] = unit_dot(shared_unit, sd_ref)
         need(ed_ref)
         expert_result(own_pieces, own_unit)
 
@@ -464,10 +476,6 @@
             relay_side(j - 1, h, dx)
         stage_pieces.append([((j - 1) * X + dx, h) for dx in range(1, X)] + [(j * X, h)])
         fillers.get(n, lambda: None)()
-        if n == stages - 1:
-            for piece in held:
-                send_result(*piece)
-            held = None
         if n >= 3:
             expert_result(stage_pieces[n - 3], stage_units[n - 3], held)
         if n == 1:
@@ -513,29 +521,29 @@
         return jnp.sum(jnp.where(lane == e, by_expert, 0.0), axis=1, keepdims=True)
 
     def mixer(i):
-        unit_wait(head_units[i])
         at = pl.ds(i * rows, rows)
-        mixer_ref[at, :] = dot(unit_rows(head_units[i]), wo_ref[...]).astype(bf16)
-
-    def add(e, got):
-        full = jnp.concatenate([got(h) for h in range(CH)], axis=0)
-        acc_ref[...] += full.astype(f32) * weight(e)
-
-    def collect(ns):
-        for n in ns:
+        mixer_ref[at, :] = unit_dot(head_units[i], wo_ref).astype(bf16)
+
+    order_weights = [weight(e) for e in order]
+
+    def collect():
+        for n in range(1, E):
             e = order[n]
             for h in range(CH):
                 remote(RO.at[n, h], RI.at[e, h], res_s.at[0], res_r.at[e, h], e, tp).wait_recv()
-            add(e, lambda h: RI[e, h])
+        for h in range(CH):
+            at = slice(h * (rows // CH), (h + 1) * (rows // CH))
+            total = acc_ref[at] + RO[0, h].astype(f32) * order_weights[0][at]
+            for n in range(1, E):
+                total += RI[order[n], h].astype(f32) * order_weights[n][at]
+            blend_ref[at, :] = total.astype(bf16)
 
     forward(last_unit)
     expert_result(last_pieces, last_unit)
-    add(ep, lambda h: RO[0, h])
     for i in range(chunks):
         forward(head_units[i])
         mixer(i)
-    collect(range(1, E))
-    blend_ref[...] = acc_ref[...].astype(bf16)
+    collect()
 
     for h in range(CH):
         pl.when(z < Z - 1)(lambda: row_up(ep, h).wait_send())
@@ -548,12 +556,13 @@
             row_x(ep, h, dx).wait_send()
             row_part(ep, h, kind).wait_send()
             for k in range(1, Z):
-                pl.when(inner(near(k)))(lambda: row_x(near(k) * X + x, h, dx).wait_send())
-                pl.when(inner(near(k)))(lambda: row_part(ep, h, kind + k).wait_send())
+                zk = near(k)
+                pl.when(by_x(zk, h))(lambda: row_x(zk * X + x, h, dx).wait_send())
+                pl.when((zk > 0) & (zk < Z - 1))(lambda: row_part(ep, h, kind + k).wait_send())
             pl.when(z < Z - 1)(lambda: row_part(ep, h, kind + Z).wait_send())
             pl.when(z > 0)(lambda: row_part(ep, h, kind + Z + 1).wait_send())
-            pl.when(z < Z - 1)(lambda: side_row(ep, h, True, dx).wait_send())
-            pl.when(z > 0)(lambda: side_row(ep, h, False, dx).wait_send())
+            pl.when(z < Z - 1 - spare(h))(lambda: side_row(ep, h, True, dx).wait_send())
+            pl.when(z > spare(h))(lambda: side_row(ep, h, False, dx).wait_send())
         pl.when(z > 0)(lambda: row_part(ep, h, 0).wait_send())
         pl.when(z < Z - 1)(lambda: row_part(ep, h, 1).wait_send())
     for sends in (part_sends, *y_sends, *f_sends, result_sends):
@@ -593,6 +602,8 @@
     chunks = seq // rows
     stages = (Z - 1) * CH
     units = 3 + stages + chunks
+    tile = min(256, width)
+    tiles = width // tile
     args = (
         queries,
         sequence_keys,
@@ -621,10 +632,10 @@
     scratch = [pltpu.VMEM(a.shape, a.dtype) for a in args]
     scratch += [
         pltpu.VMEM((experts, CH, CORES, rows // (CH * CORES), model_width), bf16),
-        pltpu.VMEM((2, lanes, rows, width), bf16),
-        pltpu.VMEM((stages, lanes, X * rows // CH, width), bf16),
-        pltpu.VMEM((1, lanes, (X - 1) * rows, width), bf16),
-        pltpu.VMEM((chunks, lanes, rows, vw), bf16),
+        pltpu.VMEM((2, lanes, tiles, rows, tile), bf16),
+        pltpu.VMEM((stages, lanes, tiles, X * rows // CH, tile), bf16),
+        pltpu.VMEM((1, lanes, tiles, (X - 1) * rows, tile), bf16),
+        pltpu.VMEM((chunks, lanes, tiles, rows, tile), bf16),
         pltpu.VMEM((experts, CH, rows // CH, outs[1].shape[1]), bf16),
         pltpu.VMEM((experts, CH, rows // CH, outs[1].shape[1]), bf16),
         pltpu.VMEM((X, DV + PAD, kw), bf16),
@@ -644,8 +655,8 @@
         dma(experts, CH),
         dma(5),
         dma(units),
-        dma(Y - 1, 9),
-        dma(Y - 1, units),
+        dma(Y - 1, 9 * tiles),
+        dma(Y - 1, units, tiles),
         dma(Y - 1, 3),
         dma(Y - 1, units),
         dma(14),

time: 53.8 us -> 52.4 us (0.974)
  Pallas kernels: 52.8 us -> 51.4 us
    pallas_call x1, Pallas kernels: 52 us -> 50.6 us  [local(): pl.pallas_call(functools.partial(body, (Z, X, Y)), out_shape=tuple((pltpu...]
where the time goes in v2:
time: 52.4 us; the launch traced here: 52.2 us
  Pallas kernels  51.4 us (98%)
  between operations  0.81 us (2%)
    pallas_call x1, Pallas kernels, local(): pl.pallas_call(functools.partial(body, (Z, X, Y)), out_shape=tuple((pltpu...  50.6 us

profile of v2, /device:TPU:0, one launch (start us, length us, event | category | flops | bytes accessed | tf_op | source)
XLA Modules:
  0.0 52.2 jit_solution(11058062812578213878)
XLA Ops:
  0.6 50.6 %step.1 = (bf16[512,512]{1,0:T(8,128)(2,1)S(1)}, bf16[128,512]{1,0:T(8,128)(2,1)S(1)}) custom-call(bf16[512,256]{1,0:T(8,128)(2,1)} %refs_0_.1, bf16[512,256]{1,0:T(8,128)(2,1)} %refs_1_.1, bf16[512,512]{1,0:T(8,128)(2,1)} %refs_2_.1, bf16[512,512]{1,0:T(8,128)(2,1)} %refs_3_.1, bf16[512,256]{1,0:T(8,128)(2,1)} %refs_4_.1, f32[512,256]{1,0:T(8,128)} %refs_5_.1, ...), custom_call_target="tpu_custom_call" | custom-call | flops 10000000000 | bytes 20971520 | tf_op jit(solution)/shard_map/step/pallas_call | solution.py:669
  51.2 0.8 %settle.1 = (bf16[512,512]{1,0:T(8,128)(2,1)}, bf16[128,512]{1,0:T(8,128)(2,1)}) custom-call(bf16[512,512]{1,0:T(8,128)(2,1)S(1)} %get-tuple-element.4.mixer_ref, bf16[128,512]{1,0:T(8,128)(2,1)S(1)} %get-tuple-element.5.blend_ref), custom_call_target="tpu_custom_call" | custom-call | flops 1000000 | bytes 2097152 | tf_op jit(solution)/shard_map/settle/pallas_call | solution.py:683

commit v3 on v2

--- a/solution.py
+++ b/solution.py
@@ -80,12 +80,27 @@
     ]
     copies = {}
 
-    def load(pairs):
-        for n, (src, dst) in enumerate(pairs):
+    def load(pairs, first=0):
+        for n, (src, dst) in enumerate(pairs, first):
             copies[id(dst)] = pltpu.make_async_copy(src, dst, in_sem.at[n])
             copies[id(dst)].start()
 
-    load(early)
+    load(early[:2])
+
+    barrier = pltpu.get_barrier_semaphore()
+
+    def greet(e, t):
+        pl.semaphore_signal(barrier, inc=1, device_id={"ep": e, "tp": t}, device_id_type=MESH)
+
+    greet(ep, partner)
+    for dy in range(1, Y):
+        greet(ep, (y + dy) % Y * CORES + c)
+    for dx in range(1, X):
+        greet(z * X + (x + dx) % X, tp)
+    pl.when(z < Z - 1)(lambda: greet(ep + X, tp))
+    pl.when(z > 0)(lambda: greet(ep - X, tp))
+
+    load(early[2:], 2)
 
     def need(*dsts):
         for dst in dsts:
@@ -107,19 +122,6 @@
             for copy in self.held.values():
                 copy.wait_send()
 
-    barrier = pltpu.get_barrier_semaphore()
-
-    def greet(e, t):
-        pl.semaphore_signal(barrier, inc=1, device_id={"ep": e, "tp": t}, device_id_type=MESH)
-
-    greet(ep, partner)
-    for dy in range(1, Y):
-        greet(ep, (y + dy) % Y * CORES + c)
-    for dx in range(1, X):
-        greet(z * X + (x + dx) % X, tp)
-    pl.when(z < Z - 1)(lambda: greet(ep + X, tp))
-    pl.when(z > 0)(lambda: greet(ep - X, tp))
-
     need(tok_ref, ng_ref)
     flat = tok_ref[...].astype(f32)
     normed = (
@@ -236,6 +238,7 @@
     def rows_of(b, h):
         return jnp.concatenate([R[b, h, n] for n in range(CORES)], axis=0)
 
+    heads_from = 3 + (Z - 1) * CH
     part_sends = Sends(u_part_s, u_part_s.shape[0])
     y_sends = [Sends(u_y_s.at[n], u_y_s.shape[1]) for n in range(Y - 1)]
     f_sends = [Sends(u_f_s.at[n], u_f_s.shape[1]) for n in range(Y - 1)]
@@ -250,7 +253,14 @@
         G, n, u = unit
         t = (y + dy) % Y * CORES + c
         sem = u_y_s.at[dy - 1, 0] if sem is None else sem
-        return remote(G.at[n, tp, m], G.at[n, tp, m], sem, u_y_r.at[dy - 1, u, m], ep, t)
+        piece = G.at[n, tp] if messages(unit) == 1 else G.at[n, tp, m]
+        return remote(piece, piece, sem, u_y_r.at[dy - 1, slot_of(u, m)], ep, t)
+
+    def slot_of(u, m):
+        return u * tiles + m if u < heads_from else heads_from * (tiles - 1) + u
+
+    def messages(unit):
+        return tiles if unit[2] < heads_from else 1
 
     def unit_f(unit, dy, sem=None):
         G, n, u = unit
@@ -261,16 +271,16 @@
     def unit_send_tile(unit, m):
         for dy in range(1, Y):
             y_sends[dy - 1].start(lambda sem: unit_y(unit, dy, m, sem))
-        if m == tiles - 1:
+        if m == messages(unit) - 1:
             part_sends.start(lambda sem: unit_part(unit, sem))
 
     def unit_send(unit):
-        for m in range(tiles):
+        for m in range(messages(unit)):
             unit_send_tile(unit, m)
 
     def unit_forward(unit):
         for dy in range(1, Y):
-            for m in range(tiles):
+            for m in range(messages(unit)):
                 unit_y(unit, dy, m).wait_recv()
             f_sends[dy - 1].start(lambda sem: unit_f(unit, dy, sem))
 
@@ -304,8 +314,11 @@
 
     def send_result(n, h):
         result_sends.start(
-            lambda sem: remote(RO.at[n, h], RI.at[ep, h], sem, res_r.at[ep, h], order[n], tp)
+            lambda sem: remote(RO.at[n, h], RI.at[ep, h], sem, res_r.at[ep], order[n], tp)
         )
+
+    def send_whole_result(n):
+        result_sends.start(lambda sem: remote(RO.at[n], RI.at[ep], sem, res_r.at[ep], order[n], tp))
 
     row = lax.broadcasted_iota(jnp.int32, (BLOCK, BLOCK), 0)
     col = lax.broadcasted_iota(jnp.int32, (BLOCK, BLOCK), 1)
@@ -415,11 +428,15 @@
         a = jnp.concatenate([rows_of(order[n], h) for n, h in pieces], axis=0)
         hidden(a, eg_ref, eu_ref, unit)
 
-    def expert_result(pieces, unit, hold=None):
+    def expert_result(pieces, unit, hold=None, whole=False):
         out = unit_dot(unit, ed_ref).astype(bf16)
         size = part * CORES
         for i, (n, h) in enumerate(pieces):
             RO[n, h] = out[i * size : (i + 1) * size]
+        if whole:
+            for n in sorted({n for n, _ in pieces}):
+                send_whole_result(n)
+            return
         for n, h in pieces:
             if n % X and hold is not None:
                 hold.append((n, h))
@@ -492,8 +509,12 @@
     for h in range(CH):
         for dx in range(1, X):
             relay_side(Z - 1, h, dx)
-    for piece in held or ():
-        send_result(*piece)
+    for n, h in held:
+        if all((n, m) in held for m in range(CH)):
+            if h == 0:
+                send_whole_result(n)
+        else:
+            send_result(n, h)
     expert_result(stage_pieces[stages - 3], stage_units[stages - 3])
     expert_hidden(last_pieces, last_unit)
     forward(stage_units[-2])
@@ -504,10 +525,10 @@
         finish(i)
         unit_send(head_units[i])
     expert_result(stage_pieces[-2], stage_units[-2])
+    forward(stage_units[-1])
     for i in range(chunks // 2, chunks):
         finish(i)
         unit_send(head_units[i])
-    forward(stage_units[-1])
     expert_result(stage_pieces[-1], stage_units[-1])
     need(wo_ref)
     need(idx_ref, w_ref)
@@ -529,8 +550,7 @@
     def collect():
         for n in range(1, E):
             e = order[n]
-            for h in range(CH):
-                remote(RO.at[n, h], RI.at[e, h], res_s.at[0], res_r.at[e, h], e, tp).wait_recv()
+            remote(RO.at[n], RI.at[e], res_s.at[0], res_r.at[e], e, tp).wait_recv()
         for h in range(CH):
             at = slice(h * (rows // CH), (h + 1) * (rows // CH))
             total = acc_ref[at] + RO[0, h].astype(f32) * order_weights[0][at]
@@ -539,7 +559,7 @@
             blend_ref[at, :] = total.astype(bf16)
 
     forward(last_unit)
-    expert_result(last_pieces, last_unit)
+    expert_result(last_pieces, last_unit, whole=True)
     for i in range(chunks):
         forward(head_units[i])
         mixer(i)
@@ -655,12 +675,12 @@
         dma(experts, CH),
         dma(5),
         dma(units),
-        dma(Y - 1, 9 * tiles),
-        dma(Y - 1, units, tiles),
+        dma(Y - 1, 10),
+        dma(Y - 1, (3 + stages) * tiles + chunks),
         dma(Y - 1, 3),
         dma(Y - 1, units),
-        dma(14),
-        dma(experts, CH),
+        dma(10),
+        dma(experts),
         dma(X - 1),
         dma(X - 1),
         dma(1),

time: 52.4 us -> 52.1 us (level)
  no operation moved by 1% of the time
where the time goes in v3:
time: 52.1 us; the launch traced here: 52 us
  Pallas kernels  51.1 us (98%)
  between operations  0.81 us (2%)
    pallas_call x1, Pallas kernels, local(): pl.pallas_call(functools.partial(body, (Z, X, Y)), out_shape=tuple((pltpu...  50.3 us

profile of v3, /device:TPU:0, one launch (start us, length us, event | category | flops | bytes accessed | tf_op | source)
XLA Modules:
  0.0 52.0 jit_solution(11563123083730561525)
XLA Ops:
  0.6 50.3 %step.1 = (bf16[512,512]{1,0:T(8,128)(2,1)S(1)}, bf16[128,512]{1,0:T(8,128)(2,1)S(1)}) custom-call(bf16[512,256]{1,0:T(8,128)(2,1)} %refs_0_.1, bf16[512,256]{1,0:T(8,128)(2,1)} %refs_1_.1, bf16[512,512]{1,0:T(8,128)(2,1)} %refs_2_.1, bf16[512,512]{1,0:T(8,128)(2,1)} %refs_3_.1, bf16[512,256]{1,0:T(8,128)(2,1)} %refs_4_.1, f32[512,256]{1,0:T(8,128)} %refs_5_.1, ...), custom_call_target="tpu_custom_call" | custom-call | flops 10000000000 | bytes 20971520 | tf_op jit(solution)/shard_map/step/pallas_call | solution.py:689
  50.9 0.8 %settle.1 = (bf16[512,512]{1,0:T(8,128)(2,1)}, bf16[128,512]{1,0:T(8,128)(2,1)}) custom-call(bf16[512,512]{1,0:T(8,128)(2,1)S(1)} %get-tuple-element.4.mixer_ref, bf16[128,512]{1,0:T(8,128)(2,1)S(1)} %get-tuple-element.5.blend_ref), custom_call_target="tpu_custom_call" | custom-call | flops 1000000 | bytes 2097152 | tf_op jit(solution)/shard_map/settle/pallas_call | solution.py:703
